TPU v7x, 128 devices: a whole 4x4x4 slice. The times are simulated.
128 devices in a mesh: sp: 16 (over z, y), tp: 8 (over x, core).
Axes of the slice: x: 4, y: 4, z: 4, core: 2. Of those that a mesh axis runs over, the one named last changes fastest.
Arguments:
- residual_in: bfloat16 [12288, 2048], P('sp', 'tp'), may hold values from -11 to 11
- queries: bfloat16 [12288, 1024], P('sp', 'tp'), may hold values from -6 to 6
- keys: bfloat16 [12288, 256], P('sp'), may hold values from -6 to 6
- values: bfloat16 [12288, 256], P('sp'), may hold values from -6 to 6
- query_gain: float32 [128], replicated, may hold values from 1.5 to 5
- key_norm_gain: float32 [128], replicated, may hold values from 1.5 to 5
- out_weight: bfloat16 [1024, 2048], P('tp'), may hold values from -0.1875 to 0.1875
- mlp_gain: float32 [2048], replicated, may hold values from 0.1 to 1.9
- gate_weight: bfloat16 [2048, 5632], P('sp', 'tp'), may hold values from -0.125 to 0.125
- up_weight: bfloat16 [2048, 5632], P('sp', 'tp'), may hold values from -0.125 to 0.125
- down_weight: bfloat16 [5632, 2048], P('tp', 'sp'), may hold values from -0.15625 to 0.15625
Outputs:
- layer_out: bfloat16 [12288, 2048], P('sp', 'tp')
All inputs are finite; a program needn't handle non-finite values.
Results may differ from a plain program's by a relative error of at most 0.012.
The roundings to bfloat16 on the way count: a program that leaves them out, or rounds other values in their place, can miss the bound.
Values may be sent and summed in bfloat16 or wider, within the bound.
A program may use at most 64 MiB of HBM per device.

v0:
```python
import jax
import jax.numpy as jnp
from jax import lax
from jax.sharding import PartitionSpec as P

D = 2048
HEAD_SIZE = 128
QUERY_HEADS = 8
KEY_VALUE_HEADS = 2
GRID = 64
eps = 1e-06
rotary_base = 10000.0


def sent_together(arrays, axis, dim, along):
    ends, at = ([], 0)
    for a in arrays[:-1]:
        at += a.shape[along]
        ends.append(at)
    both = jnp.concatenate(arrays, axis=along)
    return tuple(jnp.split(lax.all_gather(both, axis, axis=dim, tiled=True), ends, axis=along))


def laid_out(tiles, dim):
    tiles = jnp.moveaxis(tiles, 0, dim)
    lengths = tiles.shape
    return tiles.reshape(*lengths[:dim], lengths[dim] * lengths[dim + 1], *lengths[dim + 2 :])


def sent_to_all(x, axis):
    size = lax.axis_size(axis)
    return lax.all_to_all(jnp.broadcast_to(x[None], (size, *x.shape)), axis, 0, 0, tiled=True)


def gathered_copies(x, axis, dim):
    return laid_out(sent_to_all(x, axis), dim)


def taken_together(x, axis):
    everything = sent_to_all(x, axis)
    return jnp.sum(everything, axis=0)


def in_blocks(x, dim, size):
    lengths = x.shape
    tiles = x.reshape(*lengths[:dim], size, lengths[dim] // size, *lengths[dim + 1 :])
    return jnp.moveaxis(tiles, dim, 0)


def summed_on_arrival(x, axis, dim):
    tiles = in_blocks(x, dim, lax.axis_size(axis))
    arrived = lax.all_to_all(tiles, axis, split_axis=0, concat_axis=0, tiled=True)
    return arrived.astype(jnp.float32).sum(axis=0)


def apply_rotary(vectors, grid_positions):
    half_size = vectors.shape[-1] // 2
    frequency = rotary_base ** (-jnp.arange(0, half_size, 2, dtype=jnp.float32) / half_size)
    grid_row = (grid_positions // GRID).astype(jnp.float32)
    grid_col = (grid_positions % GRID).astype(jnp.float32)
    angles = jnp.concatenate(
        [grid_row[:, None] * frequency, grid_col[:, None] * frequency], axis=-1
    )[:, None, :]
    cosine_table = jnp.cos(angles)
    sine_table = jnp.sin(angles)
    first_half = vectors[..., :half_size]
    second_half = vectors[..., half_size:]
    return jnp.concatenate(
        [
            first_half * cosine_table - second_half * sine_table,
            first_half * sine_table + second_half * cosine_table,
        ],
        axis=-1,
    )


def per_head_norm(vectors, gain):
    return vectors * lax.rsqrt(jnp.mean(vectors * vectors, axis=-1, keepdims=True) + eps) * gain


def on_device(
    residual_in,
    queries,
    keys,
    values,
    query_gain,
    key_norm_gain,
    out_weight,
    mlp_gain,
    gate_weight,
    up_weight,
    down_weight,
):
    local_rows = residual_in.shape[0]
    local_heads = queries.shape[1] // HEAD_SIZE
    queries_per_group = QUERY_HEADS // KEY_VALUE_HEADS
    tp_index = lax.axis_index("tp")
    tp_count = lax.axis_size("tp")
    grid_positions = lax.axis_index("sp") * local_rows + jnp.arange(local_rows, dtype=jnp.int32)
    weight_cols = lax.all_to_all(out_weight, "tp", split_axis=1, concat_axis=0, tiled=True)
    query_rows = apply_rotary(
        per_head_norm(
            queries.astype(jnp.float32).reshape(local_rows, local_heads, HEAD_SIZE), query_gain
        ),
        grid_positions,
    ).astype(jnp.bfloat16)
    query_matrix = jnp.transpose(query_rows, (1, 0, 2)).reshape(local_heads * local_rows, HEAD_SIZE)
    shared = tp_index * local_heads // queries_per_group
    own_keys = lax.dynamic_slice_in_dim(keys, shared * HEAD_SIZE, HEAD_SIZE, 1)
    own_values = lax.dynamic_slice_in_dim(values, shared * HEAD_SIZE, HEAD_SIZE, 1)
    key_matrix = apply_rotary(
        per_head_norm(own_keys.astype(jnp.float32)[:, None, :], key_norm_gain), grid_positions
    )[:, 0, :].astype(jnp.bfloat16)
    score_scale = HEAD_SIZE ** (-0.5)
    query_count = local_heads * local_rows
    start_state = (
        jnp.full((query_count,), -1e30, jnp.float32),
        jnp.zeros((query_count,), jnp.float32),
        jnp.zeros((query_count, HEAD_SIZE), jnp.float32),
    )
    key_piece, value_piece = sent_together((key_matrix, own_values), "sp", 0, 1)
    piece_rows = key_piece.shape[0]
    block_count = -(-piece_rows // 2048)
    while piece_rows % block_count:
        block_count += 1
    block_width = piece_rows // block_count

    def one_block(block_index, state_inner):
        running_max, running_sum, weighted = state_inner
        block_keys = lax.dynamic_slice_in_dim(key_piece, block_index * block_width, block_width, 0)
        block_values = lax.dynamic_slice_in_dim(
            value_piece, block_index * block_width, block_width, 0
        )
        scores = (
            jnp.dot(query_matrix, block_keys.T, preferred_element_type=jnp.float32) * score_scale
        )
        new_max = jnp.maximum(running_max, jnp.max(scores, axis=1))
        factor = jnp.exp(running_max - new_max)
        weights = jnp.exp(scores - new_max[:, None])
        running_sum = running_sum * factor + jnp.sum(weights, axis=1)
        weighted = weighted * factor[:, None] + jnp.dot(
            weights.astype(jnp.bfloat16), block_values, preferred_element_type=jnp.float32
        )
        return (new_max, running_sum, weighted)

    running_max, running_sum, weighted = lax.fori_loop(0, block_count, one_block, start_state)
    attended = (weighted / running_sum[:, None]).astype(jnp.bfloat16)
    attended = jnp.transpose(
        attended.reshape(local_heads, local_rows, HEAD_SIZE), (1, 0, 2)
    ).reshape(local_rows, local_heads * HEAD_SIZE)
    own_width = residual_in.shape[1]
    attended_full = gathered_copies(attended, "tp", 1)
    group_width = local_heads * HEAD_SIZE
    share = jnp.zeros((local_rows, own_width), jnp.float32)
    for group_index in range(tp_count):
        left_part = attended_full[:, group_index * group_width : (group_index + 1) * group_width]
        right_part = weight_cols[group_index * group_width : (group_index + 1) * group_width, :]
        term = jnp.dot(left_part, right_part, preferred_element_type=jnp.float32).astype(
            jnp.bfloat16
        )
        share = share + term.astype(jnp.float32)
    residual_mid = residual_in.astype(jnp.float32) + share
    squares = taken_together(jnp.sum(residual_mid * residual_mid, axis=1), "tp")
    gain_own = lax.dynamic_slice_in_dim(mlp_gain, tp_index * own_width, own_width, 0)
    normed_own = (residual_mid * lax.rsqrt(squares / D + eps)[:, None] * gain_own).astype(
        jnp.bfloat16
    )
    normed = lax.all_gather(normed_own, "tp", axis=1, tiled=True)
    pieces = sent_together((gate_weight, up_weight), "sp", 0, 1)
    gate_out = jnp.dot(normed, pieces[0], preferred_element_type=jnp.float32)
    up_out = jnp.dot(normed, pieces[1], preferred_element_type=jnp.float32)
    hidden = (jax.nn.silu(gate_out) * up_out).astype(jnp.bfloat16)
    down_terms = jnp.dot(
        hidden,
        lax.all_gather(down_weight, "sp", axis=1, tiled=True),
        preferred_element_type=jnp.float32,
    )
    down_share = summed_on_arrival(down_terms.astype(jnp.bfloat16), "tp", 1)
    return (residual_mid + 0.5 * down_share).astype(jnp.bfloat16)


def solution(mesh):
    in_specs = (
        P("sp", "tp"),
        P("sp", "tp"),
        P("sp", None),
        P("sp", None),
        P(),
        P(),
        P("tp", None),
        P(),
        P("sp", "tp"),
        P("sp", "tp"),
        P("tp", "sp"),
    )
    out_specs = P("sp", "tp")
    return jax.shard_map(
        on_device, mesh=mesh, in_specs=in_specs, out_specs=out_specs, check_vma=False
    )
```

profile of v0, /device:TPU:1, one launch (start us, length us, event | category | flops | bytes accessed | tf_op | source)
XLA Modules:
  0.0 336.8 jit_solution(7837900333065985362)
XLA Ops:
  14.6 5.8 %all-to-all-start.1 = ((bf16[128,8,256]{0,2,1:T(8,128)(2,1)}), bf16[128,8,256]{0,2,1:T(8,128)(2,1)S(1)}, u32[]{:S(2)}, u32[]{:S(2)}) async-start(bf16[128,8,256]{0,2,1:T(8,128)(2,1)} %bitcast.9), calls=%async_computation.1 | async-start | bytes 1048576 | tf_op jit(solution)/shard_map/all_to_all | solution.py:100
  21.4 56.8 %all-gather.5.cloned.1.call-done = bf16[12288,256]{1,0:T(8,128)(2,1)} async-done(((bf16[768,256]{1,0:T(8,128)(2,1)}), bf16[12288,256]{1,0:T(8,128)(2,1)}) %all-gather.5.cloned.1.call-update) | async-done | bytes 6291472 | tf_op jit(solution)/shard_map/all_gather | solution.py:21
  78.2 4.7 %fusion.66 = (bf16[12288,128]{1,0:T(8,128)(2,1)}, bf16[12288,128]{1,0:T(8,128)(2,1)}) fusion(bf16[12288,256]{1,0:T(8,128)(2,1)} %all-gather.5.cloned.1.call-done), kind=kLoop, calls=%fused_computation.114 | loop fusion | bytes 12582912 | tf_op jit(solution)/shard_map/split | solution.py:21
  82.9 71.6 %while.18 = (s32[]{:T(128)}, f32[768]{0:T(1024)S(1)}, f32[768]{0:T(1024)S(1)}, f32[768,128]{1,0:T(8,128)S(1)}, bf16[12288,128]{1,0:T(8,128)(2,1)}, /*index=5*/bf...) while((s32[]{:T(128)}, f32[768]{0:T(1024)S(1)}, ...), condition=%wide.region_5.6_spmd.clone, body=%wide.region_2.5_spmd.clone.sunk | while | flops 818188032 | bytes 46121160 | solution.py:146
  82.9 4.7 %multiply_reduce_fusion.3 = (f32[768]{0:T(1024)S(1)}, f32[2048,768]{1,0:T(8,128)}) fusion(bf16[768,128]{1,0:T(8,128)(2,1)S(1)} %get-tuple-element.268, bf16[12288,128]{1,0:T(8,128)(2,1)} %get-tuple-element.267, s32[]{:T(128)S(6)} %select_n.55), kind=kOutput, calls=%fused_computation.1.clone.1 | convolution fusion | flops 405798144 | bytes 7015428 | tf_op jit(solution)/shard_map/while/body/eval_jaxpr/dot_general | solution.py:135
  87.6 4.2 %fusion.80 = f32[768]{0:T(1024)S(1)} fusion(f32[2048,768]{1,0:T(8,128)} %get-tuple-element.238, f32[768]{0:T(1024)S(1)} %select_maximum_fusion.2), kind=kLoop, calls=%fused_computation.3.clone.1 | loop fusion | flops 4717824 | bytes 6297600 | tf_op jit(solution)/shard_map/while/body/eval_jaxpr/reduce_sum | solution.py:140
  92.6 2.4 fusion.82
  95.0 4.7 %multiply_reduce_fusion.3 = (f32[768]{0:T(1024)S(1)}, f32[2048,768]{1,0:T(8,128)}) fusion(bf16[768,128]{1,0:T(8,128)(2,1)S(1)} %get-tuple-element.268, bf16[12288,128]{1,0:T(8,128)(2,1)} %get-tuple-element.267, s32[]{:T(128)S(6)} %select_n.55), kind=kOutput, calls=%fused_computation.1.clone.1 | convolution fusion | flops 405798144 | bytes 7015428 | tf_op jit(solution)/shard_map/while/body/eval_jaxpr/dot_general | solution.py:135
  99.6 4.1 %fusion.80 = f32[768]{0:T(1024)S(1)} fusion(f32[2048,768]{1,0:T(8,128)} %get-tuple-element.238, f32[768]{0:T(1024)S(1)} %select_maximum_fusion.2), kind=kLoop, calls=%fused_computation.3.clone.1 | loop fusion | flops 4717824 | bytes 6297600 | tf_op jit(solution)/shard_map/while/body/eval_jaxpr/reduce_sum | solution.py:140
  104.3 2.4 fusion.82
  106.7 4.7 %multiply_reduce_fusion.3 = (f32[768]{0:T(1024)S(1)}, f32[2048,768]{1,0:T(8,128)}) fusion(bf16[768,128]{1,0:T(8,128)(2,1)S(1)} %get-tuple-element.268, bf16[12288,128]{1,0:T(8,128)(2,1)} %get-tuple-element.267, s32[]{:T(128)S(6)} %select_n.55), kind=kOutput, calls=%fused_computation.1.clone.1 | convolution fusion | flops 405798144 | bytes 7015428 | tf_op jit(solution)/shard_map/while/body/eval_jaxpr/dot_general | solution.py:135
  111.4 4.2 %fusion.80 = f32[768]{0:T(1024)S(1)} fusion(f32[2048,768]{1,0:T(8,128)} %get-tuple-element.238, f32[768]{0:T(1024)S(1)} %select_maximum_fusion.2), kind=kLoop, calls=%fused_computation.3.clone.1 | loop fusion | flops 4717824 | bytes 6297600 | tf_op jit(solution)/shard_map/while/body/eval_jaxpr/reduce_sum | solution.py:140
  116.4 2.4 fusion.82
  118.8 4.7 %multiply_reduce_fusion.3 = (f32[768]{0:T(1024)S(1)}, f32[2048,768]{1,0:T(8,128)}) fusion(bf16[768,128]{1,0:T(8,128)(2,1)S(1)} %get-tuple-element.268, bf16[12288,128]{1,0:T(8,128)(2,1)} %get-tuple-element.267, s32[]{:T(128)S(6)} %select_n.55), kind=kOutput, calls=%fused_computation.1.clone.1 | convolution fusion | flops 405798144 | bytes 7015428 | tf_op jit(solution)/shard_map/while/body/eval_jaxpr/dot_general | solution.py:135
  123.5 4.2 %fusion.80 = f32[768]{0:T(1024)S(1)} fusion(f32[2048,768]{1,0:T(8,128)} %get-tuple-element.238, f32[768]{0:T(1024)S(1)} %select_maximum_fusion.2), kind=kLoop, calls=%fused_computation.3.clone.1 | loop fusion | flops 4717824 | bytes 6297600 | tf_op jit(solution)/shard_map/while/body/eval_jaxpr/reduce_sum | solution.py:140
  128.5 2.4 fusion.82
  130.9 4.7 %multiply_reduce_fusion.3 = (f32[768]{0:T(1024)S(1)}, f32[2048,768]{1,0:T(8,128)}) fusion(bf16[768,128]{1,0:T(8,128)(2,1)S(1)} %get-tuple-element.268, bf16[12288,128]{1,0:T(8,128)(2,1)} %get-tuple-element.267, s32[]{:T(128)S(6)} %select_n.55), kind=kOutput, calls=%fused_computation.1.clone.1 | convolution fusion | flops 405798144 | bytes 7015428 | tf_op jit(solution)/shard_map/while/body/eval_jaxpr/dot_general | solution.py:135
  135.6 4.2 %fusion.80 = f32[768]{0:T(1024)S(1)} fusion(f32[2048,768]{1,0:T(8,128)} %get-tuple-element.238, f32[768]{0:T(1024)S(1)} %select_maximum_fusion.2), kind=kLoop, calls=%fused_computation.3.clone.1 | loop fusion | flops 4717824 | bytes 6297600 | tf_op jit(solution)/shard_map/while/body/eval_jaxpr/reduce_sum | solution.py:140
  140.5 2.4 fusion.82
  142.9 4.7 %multiply_reduce_fusion.3 = (f32[768]{0:T(1024)S(1)}, f32[2048,768]{1,0:T(8,128)}) fusion(bf16[768,128]{1,0:T(8,128)(2,1)S(1)} %get-tuple-element.268, bf16[12288,128]{1,0:T(8,128)(2,1)} %get-tuple-element.267, s32[]{:T(128)S(6)} %select_n.55), kind=kOutput, calls=%fused_computation.1.clone.1 | convolution fusion | flops 405798144 | bytes 7015428 | tf_op jit(solution)/shard_map/while/body/eval_jaxpr/dot_general | solution.py:135
  147.5 4.0 %fusion.80 = f32[768]{0:T(1024)S(1)} fusion(f32[2048,768]{1,0:T(8,128)} %get-tuple-element.238, f32[768]{0:T(1024)S(1)} %select_maximum_fusion.2), kind=kLoop, calls=%fused_computation.3.clone.1 | loop fusion | flops 4717824 | bytes 6297600 | tf_op jit(solution)/shard_map/while/body/eval_jaxpr/reduce_sum | solution.py:140
  152.1 2.4 fusion.82
  156.2 5.2 %all-to-all-start = ((bf16[8,768,128]{1,2,0:T(8,128)(2,1)}), bf16[8,768,128]{1,2,0:T(8,128)(2,1)S(1)}, u32[]{:S(2)}, u32[]{:S(2)}) async-start(bf16[8,768,128]{1,2,0:T(8,128)(2,1)} %broadcast_in_dim.17), calls=%async_computation | async-start | bytes 3145728 | tf_op jit(solution)/shard_map/all_to_all | solution.py:32
  163.3 18.7 %all-to-all-done = bf16[8,768,128]{1,2,0:T(8,128)(2,1)S(1)} async-done(((bf16[8,768,128]{1,2,0:T(8,128)(2,1)}), bf16[8,768,128]{1,2,0:T(8,128)(2,1)S(1)}, u32[]{:S(2)}, u32[]{:S(2)}) %all-to-all-start) | async-done | bytes 1572896 | tf_op jit(solution)/shard_map/all_to_all | solution.py:32
  184.9 4.2 %all-to-all-start.2 = ((f32[8,1,768]{2,1,0:T(1,128)}), f32[8,1,768]{2,1,0:T(1,128)S(1)}, u32[]{:S(2)}, u32[]{:S(2)}) async-start(f32[8,1,768]{2,1,0:T(1,128)} %broadcast_in_dim.18), calls=%async_computation.2 | async-start | bytes 49152 | tf_op jit(solution)/shard_map/all_to_all | solution.py:32
  189.9 3.9 %all-to-all-done.2 = f32[8,1,768]{2,1,0:T(1,128)S(1)} async-done(((f32[8,1,768]{2,1,0:T(1,128)}), f32[8,1,768]{2,1,0:T(1,128)S(1)}, u32[]{:S(2)}, u32[]{:S(2)}) %all-to-all-start.2) | async-done | bytes 24608 | tf_op jit(solution)/shard_map/all_to_all | solution.py:32
  195.3 24.9 %all-gather.7.cloned.1.call-done = bf16[768,2048]{0,1:T(8,128)(2,1)} async-done(((bf16[768,256]{0,1:T(8,128)(2,1)}), bf16[768,2048]{0,1:T(8,128)(2,1)}) %all-gather.7.cloned.1.call-update) | async-done | bytes 3145744 | tf_op jit(solution)/shard_map/all_gather | solution.py:168
  220.2 5.2 %fusion.16 = f32[768,704]{0,1:T(8,128)S(1)} fusion(bf16[768,2048]{0,1:T(8,128)(2,1)} %all-gather.7.cloned.1.call-done, bf16[2048,1408]{0,1:T(8,128)(2,1)} %all-gather.9.cloned.1.call-done), kind=kOutput, calls=%fused_computation.22 | convolution fusion | flops 2214592512 | bytes 8192000 | tf_op jit(solution)/shard_map/dot_general | solution.py:170
  225.4 45.8 %all-gather.11.cloned.1.call-done = bf16[704,2048]{1,0:T(8,128)(2,1)} async-done(((bf16[704,128]{1,0:T(8,128)(2,1)}), bf16[704,2048]{1,0:T(8,128)(2,1)}) %all-gather.11.cloned.1.call-update) | async-done | bytes 2883600 | tf_op jit(solution)/shard_map/all_gather | solution.py:175
  271.2 11.7 %convolution_convert_fusion = bf16[768,2048]{1,0:T(8,128)(2,1)} fusion(bf16[704,2048]{1,0:T(8,128)(2,1)} %all-gather.11.cloned.1.call-done, f32[768,704]{0,1:T(8,128)S(1)} %fusion.16, bf16[768,2048]{0,1:T(8,128)(2,1)} %all-gather.7.cloned.1.call-done, bf16[2048,1408]{0,1:T(8,128)(2,1)} %all-gather.9.cloned.1.call-done), kind=kOutput, calls=%fused_computation.18 | convolution fusion | flops 4434001920 | bytes 14221312 | tf_op jit(solution)/shard_map/dot_general | solution.py:173
  282.9 2.1 copy.79
  285.0 43.5 %all_to_all.32 = bf16[8,768,256]{2,1,0:T(8,128)(2,1)S(1)} all-to-all(bf16[8,768,256]{2,1,0:T(8,128)(2,1)S(1)} %bitcast.66), channel_id=1, replica_groups=mesh['sp'=16,'tp'=8] {'tp'}, dimensions={0} | all-to-all | bytes 6291456 | tf_op jit(solution)/shard_map/all_to_all | solution.py:52
  (90 shorter events, 23.5 us)
Async XLA Ops:
  6.5 2.4 copy-start
  6.5 71.7 %all-gather.5.cloned.1.call-start = ((), (), s32[]{:S(2)}) async-start(), calls=%async_computation.4 | async-start | bytes 6684672 | tf_op jit(solution)/shard_map/all_gather | solution.py:21
  10.5 3.1 copy-start.3
  12.3 8.1 %copy-start.4 = (bf16[128,704]{0,1:T(8,128)(2,1)S(1)}, bf16[128,704]{0,1:T(8,128)(2,1)}, u32[]{:S(2)}) copy-start(bf16[128,704]{0,1:T(8,128)(2,1)} %param.22) | copy-start | bytes 540676
  12.3 8.1 %copy-start.5 = (bf16[128,704]{0,1:T(8,128)(2,1)S(1)}, bf16[128,704]{0,1:T(8,128)(2,1)}, u32[]{:S(2)}) copy-start(bf16[128,704]{0,1:T(8,128)(2,1)} %param.21) | copy-start | bytes 540676
  14.6 140.2 %all-to-all-start.1 = ((bf16[128,8,256]{0,2,1:T(8,128)(2,1)}), bf16[128,8,256]{0,2,1:T(8,128)(2,1)S(1)}, u32[]{:S(2)}, u32[]{:S(2)}) async-start(bf16[128,8,256]{0,2,1:T(8,128)(2,1)} %bitcast.9), calls=%async_computation.1 | async-start | bytes 1048576 | tf_op jit(solution)/shard_map/all_to_all | solution.py:100
  20.4 174.9 %all-gather.9.cloned.1.call-start = ((), (), s32[]{:S(2)}) async-start(), calls=%async_computation.6 | async-start | bytes 6127616 | tf_op jit(solution)/shard_map/all_gather | solution.py:21
  87.6 5.0 %copy-start.1 = (f32[2048,768]{1,0:T(8,128)S(1)}, f32[2048,768]{1,0:T(8,128)}, u32[]{:S(2)}) copy-start(f32[2048,768]{1,0:T(8,128)} %get-tuple-element.238) | copy-start | bytes 18874372 | tf_op jit(solution)/shard_map/while
  99.6 4.7 %copy-start.1 = (f32[2048,768]{1,0:T(8,128)S(1)}, f32[2048,768]{1,0:T(8,128)}, u32[]{:S(2)}) copy-start(f32[2048,768]{1,0:T(8,128)} %get-tuple-element.238) | copy-start | bytes 18874372 | tf_op jit(solution)/shard_map/while
  111.4 5.0 %copy-start.1 = (f32[2048,768]{1,0:T(8,128)S(1)}, f32[2048,768]{1,0:T(8,128)}, u32[]{:S(2)}) copy-start(f32[2048,768]{1,0:T(8,128)} %get-tuple-element.238) | copy-start | bytes 18874372 | tf_op jit(solution)/shard_map/while
  123.5 5.0 %copy-start.1 = (f32[2048,768]{1,0:T(8,128)S(1)}, f32[2048,768]{1,0:T(8,128)}, u32[]{:S(2)}) copy-start(f32[2048,768]{1,0:T(8,128)} %get-tuple-element.238) | copy-start | bytes 18874372 | tf_op jit(solution)/shard_map/while
  135.6 4.9 %copy-start.1 = (f32[2048,768]{1,0:T(8,128)S(1)}, f32[2048,768]{1,0:T(8,128)}, u32[]{:S(2)}) copy-start(f32[2048,768]{1,0:T(8,128)} %get-tuple-element.238) | copy-start | bytes 18874372 | tf_op jit(solution)/shard_map/while
  147.5 4.6 %copy-start.1 = (f32[2048,768]{1,0:T(8,128)S(1)}, f32[2048,768]{1,0:T(8,128)}, u32[]{:S(2)}) copy-start(f32[2048,768]{1,0:T(8,128)} %get-tuple-element.238) | copy-start | bytes 18874372 | tf_op jit(solution)/shard_map/while
  156.2 25.8 %all-to-all-start = ((bf16[8,768,128]{1,2,0:T(8,128)(2,1)}), bf16[8,768,128]{1,2,0:T(8,128)(2,1)S(1)}, u32[]{:S(2)}, u32[]{:S(2)}) async-start(bf16[8,768,128]{1,2,0:T(8,128)(2,1)} %broadcast_in_dim.17), calls=%async_computation | async-start | bytes 3145728 | tf_op jit(solution)/shard_map/all_to_all | solution.py:32
  183.0 1.0 copy-start.2
  184.9 8.9 %all-to-all-start.2 = ((f32[8,1,768]{2,1,0:T(1,128)}), f32[8,1,768]{2,1,0:T(1,128)S(1)}, u32[]{:S(2)}, u32[]{:S(2)}) async-start(f32[8,1,768]{2,1,0:T(1,128)} %broadcast_in_dim.18), calls=%async_computation.2 | async-start | bytes 49152 | tf_op jit(solution)/shard_map/all_to_all | solution.py:32
  189.1 31.1 %all-gather.7.cloned.1.call-start = ((), (), s32[]{:S(2)}) async-start(), calls=%async_computation.5 | async-start | bytes 3538944 | tf_op jit(solution)/shard_map/all_gather | solution.py:168
  194.7 76.4 %all-gather.11.cloned.1.call-start = ((), (), s32[]{:S(2)}) async-start(), calls=%async_computation.7 | async-start | bytes 3063808 | tf_op jit(solution)/shard_map/all_gather | solution.py:175
Sparse Core Ops, SparseCore 0:
  13.7 64.4 all-gather.4
  80.3 62.8 all-gather.8
  194.9 25.3 all-gather.6
  222.2 48.9 all-gather.10
where the time goes:
time: 338 us; the launch traced here: 337 us
  waiting for transfers between devices  151 us (45%)
  matrix products  61.1 us (18%)
  blocking collectives  43.5 us (13%)
  other arithmetic  34.3 us (10%)
  local copies, waits for them, and re-layouts  18.2 us (5%)
  starting transfers between devices  15.5 us (5%)
  between operations  13.4 us (4%)
    all_gather x2, waiting for transfers between devices, sent_together(): lax.all_gather(both, axis, axis=dim, tiled=True)  56.8 us
    all_gather x1, waiting for transfers between devices, on_device(): lax.all_gather(down_weight, 'sp', axis=1, tiled=True)  45.8 us
    all_to_all x1, blocking collectives, summed_on_arrival(): lax.all_to_all(tiles, axis, split_axis=0, concat_axis=0, tiled=True)  43.5 us
    dot_general x6, matrix products, one_block(): jnp.dot(query_matrix, block_keys.T, preferred_element_type=jnp.float32)  28 us
    all_gather x1, waiting for transfers between devices, on_device(): normed = lax.all_gather(normed_own, 'tp', axis=1, tiled=True)  24.9 us
    reduce_sum x6, other arithmetic, one_block(): running_sum = running_sum * factor + jnp.sum(weights, axis=1)  24.8 us
    all_to_all x2, waiting for transfers between devices, sent_to_all(): lax.all_to_all(jnp.broadcast_to(x[None], (size, *x.shape)), axis, 0, 0, t...  22.6 us
    dot_general x6, matrix products, one_block(): jnp.dot(weights.astype(jnp.bfloat16), block_values, preferred_element_typ...  14.2 us
  transfers between devices with their start and end apart: 7, of which 5 were waited for; matrix products, arithmetic and copies ran while one was open for 26% of the time, Pallas kernels for 0%

commit v1 on v0

--- a/solution.py
+++ b/solution.py
@@ -172,7 +172,9 @@
     hidden = (jax.nn.silu(gate_out) * up_out).astype(jnp.bfloat16)
     down_terms = jnp.dot(
         hidden,
-        lax.all_gather(down_weight, "sp", axis=1, tiled=True),
+        jnp.concatenate(
+            lax.all_to_all(jnp.stack([down_weight] * lax.axis_size("sp")), "sp", 0, 0), axis=1
+        ),
         preferred_element_type=jnp.float32,
     )
     down_share = summed_on_arrival(down_terms.astype(jnp.bfloat16), "tp", 1)

time: 338 us -> 309 us (0.914)
  waiting for transfers between devices: 151 us -> 117 us
  starting transfers between devices: 15.5 us -> 19.9 us
    all_gather x1 -> x0, waiting for transfers between devices: 45.8 us -> none  [on_device(): lax.all_gather(down_weight, 'sp', axis=1, tiled=True)]
    all_to_all x0 -> x1, waiting for transfers between devices: none -> 18.9 us  [on_device(): lax.all_to_all(jnp.stack([down_weight] * lax.axis_size('sp')), 'sp', 0, 0)]
    all_gather x1, waiting for transfers between devices: 24.9 us -> 18.6 us  [on_device(): normed = lax.all_gather(normed_own, 'tp', axis=1, tiled=True)]
    all_to_all x0 -> x1, starting transfers between devices: none -> 4.67 us  [on_device(): lax.all_to_all(jnp.stack([down_weight] * lax.axis_size('sp')), 'sp', 0, 0)]
  transfers between devices with their start and end apart: 7 -> 7, of which waited for: 5 -> 5; matrix products, arithmetic and copies ran while one was open for 26% -> 29% of each run, Pallas kernels for 0% -> 0%
where the time goes in v1:
time: 309 us; the launch traced here: 308 us
  waiting for transfers between devices  117 us (38%)
  matrix products  61.2 us (20%)
  blocking collectives  41.7 us (13%)
  other arithmetic  34.3 us (11%)
  local copies, waits for them, and re-layouts  20.4 us (7%)
  starting transfers between devices  19.9 us (6%)
  between operations  13.4 us (4%)
    all_gather x2, waiting for transfers between devices, sent_together(): lax.all_gather(both, axis, axis=dim, tiled=True)  56.8 us
    all_to_all x1, blocking collectives, summed_on_arrival(): lax.all_to_all(tiles, axis, split_axis=0, concat_axis=0, tiled=True)  41.7 us
    dot_general x6, matrix products, one_block(): jnp.dot(query_matrix, block_keys.T, preferred_element_type=jnp.float32)  28 us
    reduce_sum x6, other arithmetic, one_block(): running_sum = running_sum * factor + jnp.sum(weights, axis=1)  24.8 us
    all_to_all x2, waiting for transfers between devices, sent_to_all(): lax.all_to_all(jnp.broadcast_to(x[None], (size, *x.shape)), axis, 0, 0, t...  22.6 us
    all_to_all x1, waiting for transfers between devices, on_device(): lax.all_to_all(jnp.stack([down_weight] * lax.axis_size('sp')), 'sp', 0, 0)  18.9 us
    all_gather x1, waiting for transfers between devices, on_device(): normed = lax.all_gather(normed_own, 'tp', axis=1, tiled=True)  18.6 us
    dot_general x6, matrix products, one_block(): jnp.dot(weights.astype(jnp.bfloat16), block_values, preferred_element_typ...  14.2 us
  transfers between devices with their start and end apart: 7, of which 5 were waited for; matrix products, arithmetic and copies ran while one was open for 29% of the time, Pallas kernels for 0%

profile of v1, /device:TPU:1, one launch (start us, length us, event | category | flops | bytes accessed | tf_op | source)
XLA Modules:
  0.0 308.1 jit_solution(12489241211388810813)
XLA Ops:
  14.6 5.8 %all-to-all-start.1 = ((bf16[128,8,256]{0,2,1:T(8,128)(2,1)}), bf16[128,8,256]{0,2,1:T(8,128)(2,1)S(1)}, u32[]{:S(2)}, u32[]{:S(2)}) async-start(bf16[128,8,256]{0,2,1:T(8,128)(2,1)} %bitcast.9), calls=%async_computation.1 | async-start | bytes 1048576 | tf_op jit(solution)/shard_map/all_to_all | solution.py:100
  21.4 56.8 %all-gather.4.cloned.1.call-done = bf16[12288,256]{1,0:T(8,128)(2,1)} async-done(((bf16[768,256]{1,0:T(8,128)(2,1)}), bf16[12288,256]{1,0:T(8,128)(2,1)}) %all-gather.4.cloned.1.call-update) | async-done | bytes 6291472 | tf_op jit(solution)/shard_map/all_gather | solution.py:21
  78.2 4.7 %fusion.68 = (bf16[12288,128]{1,0:T(8,128)(2,1)}, bf16[12288,128]{1,0:T(8,128)(2,1)}) fusion(bf16[12288,256]{1,0:T(8,128)(2,1)} %all-gather.4.cloned.1.call-done), kind=kLoop, calls=%fused_computation.116 | loop fusion | bytes 12582912 | tf_op jit(solution)/shard_map/split | solution.py:21
  82.9 71.6 %while.18 = (s32[]{:T(128)}, f32[768]{0:T(1024)S(1)}, f32[768]{0:T(1024)S(1)}, f32[768,128]{1,0:T(8,128)S(1)}, bf16[12288,128]{1,0:T(8,128)(2,1)}, /*index=5*/bf...) while((s32[]{:T(128)}, f32[768]{0:T(1024)S(1)}, ...), condition=%wide.region_5.6_spmd.clone, body=%wide.region_2.5_spmd.clone.sunk | while | flops 818188032 | bytes 46121160 | solution.py:146
  82.9 4.7 %multiply_reduce_fusion.3 = (f32[768]{0:T(1024)S(1)}, f32[2048,768]{1,0:T(8,128)}) fusion(bf16[768,128]{1,0:T(8,128)(2,1)S(1)} %get-tuple-element.268, bf16[12288,128]{1,0:T(8,128)(2,1)} %get-tuple-element.267, s32[]{:T(128)S(6)} %select_n.55), kind=kOutput, calls=%fused_computation.1.clone.1 | convolution fusion | flops 405798144 | bytes 7015428 | tf_op jit(solution)/shard_map/while/body/eval_jaxpr/dot_general | solution.py:135
  87.6 4.2 %fusion.82 = f32[768]{0:T(1024)S(1)} fusion(f32[2048,768]{1,0:T(8,128)} %get-tuple-element.238, f32[768]{0:T(1024)S(1)} %select_maximum_fusion.2), kind=kLoop, calls=%fused_computation.3.clone.1 | loop fusion | flops 4717824 | bytes 6297600 | tf_op jit(solution)/shard_map/while/body/eval_jaxpr/reduce_sum | solution.py:140
  92.6 2.4 fusion.84
  95.0 4.7 %multiply_reduce_fusion.3 = (f32[768]{0:T(1024)S(1)}, f32[2048,768]{1,0:T(8,128)}) fusion(bf16[768,128]{1,0:T(8,128)(2,1)S(1)} %get-tuple-element.268, bf16[12288,128]{1,0:T(8,128)(2,1)} %get-tuple-element.267, s32[]{:T(128)S(6)} %select_n.55), kind=kOutput, calls=%fused_computation.1.clone.1 | convolution fusion | flops 405798144 | bytes 7015428 | tf_op jit(solution)/shard_map/while/body/eval_jaxpr/dot_general | solution.py:135
  99.6 4.1 %fusion.82 = f32[768]{0:T(1024)S(1)} fusion(f32[2048,768]{1,0:T(8,128)} %get-tuple-element.238, f32[768]{0:T(1024)S(1)} %select_maximum_fusion.2), kind=kLoop, calls=%fused_computation.3.clone.1 | loop fusion | flops 4717824 | bytes 6297600 | tf_op jit(solution)/shard_map/while/body/eval_jaxpr/reduce_sum | solution.py:140
  104.3 2.4 fusion.84
  106.7 4.7 %multiply_reduce_fusion.3 = (f32[768]{0:T(1024)S(1)}, f32[2048,768]{1,0:T(8,128)}) fusion(bf16[768,128]{1,0:T(8,128)(2,1)S(1)} %get-tuple-element.268, bf16[12288,128]{1,0:T(8,128)(2,1)} %get-tuple-element.267, s32[]{:T(128)S(6)} %select_n.55), kind=kOutput, calls=%fused_computation.1.clone.1 | convolution fusion | flops 405798144 | bytes 7015428 | tf_op jit(solution)/shard_map/while/body/eval_jaxpr/dot_general | solution.py:135
  111.4 4.2 %fusion.82 = f32[768]{0:T(1024)S(1)} fusion(f32[2048,768]{1,0:T(8,128)} %get-tuple-element.238, f32[768]{0:T(1024)S(1)} %select_maximum_fusion.2), kind=kLoop, calls=%fused_computation.3.clone.1 | loop fusion | flops 4717824 | bytes 6297600 | tf_op jit(solution)/shard_map/while/body/eval_jaxpr/reduce_sum | solution.py:140
  116.4 2.4 fusion.84
  118.8 4.7 %multiply_reduce_fusion.3 = (f32[768]{0:T(1024)S(1)}, f32[2048,768]{1,0:T(8,128)}) fusion(bf16[768,128]{1,0:T(8,128)(2,1)S(1)} %get-tuple-element.268, bf16[12288,128]{1,0:T(8,128)(2,1)} %get-tuple-element.267, s32[]{:T(128)S(6)} %select_n.55), kind=kOutput, calls=%fused_computation.1.clone.1 | convolution fusion | flops 405798144 | bytes 7015428 | tf_op jit(solution)/shard_map/while/body/eval_jaxpr/dot_general | solution.py:135
  123.5 4.2 %fusion.82 = f32[768]{0:T(1024)S(1)} fusion(f32[2048,768]{1,0:T(8,128)} %get-tuple-element.238, f32[768]{0:T(1024)S(1)} %select_maximum_fusion.2), kind=kLoop, calls=%fused_computation.3.clone.1 | loop fusion | flops 4717824 | bytes 6297600 | tf_op jit(solution)/shard_map/while/body/eval_jaxpr/reduce_sum | solution.py:140
  128.5 2.4 fusion.84
  130.9 4.7 %multiply_reduce_fusion.3 = (f32[768]{0:T(1024)S(1)}, f32[2048,768]{1,0:T(8,128)}) fusion(bf16[768,128]{1,0:T(8,128)(2,1)S(1)} %get-tuple-element.268, bf16[12288,128]{1,0:T(8,128)(2,1)} %get-tuple-element.267, s32[]{:T(128)S(6)} %select_n.55), kind=kOutput, calls=%fused_computation.1.clone.1 | convolution fusion | flops 405798144 | bytes 7015428 | tf_op jit(solution)/shard_map/while/body/eval_jaxpr/dot_general | solution.py:135
  135.6 4.2 %fusion.82 = f32[768]{0:T(1024)S(1)} fusion(f32[2048,768]{1,0:T(8,128)} %get-tuple-element.238, f32[768]{0:T(1024)S(1)} %select_maximum_fusion.2), kind=kLoop, calls=%fused_computation.3.clone.1 | loop fusion | flops 4717824 | bytes 6297600 | tf_op jit(solution)/shard_map/while/body/eval_jaxpr/reduce_sum | solution.py:140
  140.5 2.4 fusion.84
  142.9 4.7 %multiply_reduce_fusion.3 = (f32[768]{0:T(1024)S(1)}, f32[2048,768]{1,0:T(8,128)}) fusion(bf16[768,128]{1,0:T(8,128)(2,1)S(1)} %get-tuple-element.268, bf16[12288,128]{1,0:T(8,128)(2,1)} %get-tuple-element.267, s32[]{:T(128)S(6)} %select_n.55), kind=kOutput, calls=%fused_computation.1.clone.1 | convolution fusion | flops 405798144 | bytes 7015428 | tf_op jit(solution)/shard_map/while/body/eval_jaxpr/dot_general | solution.py:135
  147.5 4.0 %fusion.82 = f32[768]{0:T(1024)S(1)} fusion(f32[2048,768]{1,0:T(8,128)} %get-tuple-element.238, f32[768]{0:T(1024)S(1)} %select_maximum_fusion.2), kind=kLoop, calls=%fused_computation.3.clone.1 | loop fusion | flops 4717824 | bytes 6297600 | tf_op jit(solution)/shard_map/while/body/eval_jaxpr/reduce_sum | solution.py:140
  152.1 2.4 fusion.84
  156.2 5.2 %all-to-all-start = ((bf16[8,768,128]{1,2,0:T(8,128)(2,1)}), bf16[8,768,128]{1,2,0:T(8,128)(2,1)S(1)}, u32[]{:S(2)}, u32[]{:S(2)}) async-start(bf16[8,768,128]{1,2,0:T(8,128)(2,1)} %broadcast_in_dim.17), calls=%async_computation | async-start | bytes 3145728 | tf_op jit(solution)/shard_map/all_to_all | solution.py:32
  163.3 18.7 %all-to-all-done = bf16[8,768,128]{1,2,0:T(8,128)(2,1)S(1)} async-done(((bf16[8,768,128]{1,2,0:T(8,128)(2,1)}), bf16[8,768,128]{1,2,0:T(8,128)(2,1)S(1)}, u32[]{:S(2)}, u32[]{:S(2)}) %all-to-all-start) | async-done | bytes 1572896 | tf_op jit(solution)/shard_map/all_to_all | solution.py:32
  184.9 4.2 %all-to-all-start.2 = ((f32[8,1,768]{2,1,0:T(1,128)}), f32[8,1,768]{2,1,0:T(1,128)S(1)}, u32[]{:S(2)}, u32[]{:S(2)}) async-start(f32[8,1,768]{2,1,0:T(1,128)} %broadcast_in_dim.18), calls=%async_computation.2 | async-start | bytes 49152 | tf_op jit(solution)/shard_map/all_to_all | solution.py:32
  189.9 3.9 %all-to-all-done.2 = f32[8,1,768]{2,1,0:T(1,128)S(1)} async-done(((f32[8,1,768]{2,1,0:T(1,128)}), f32[8,1,768]{2,1,0:T(1,128)S(1)}, u32[]{:S(2)}, u32[]{:S(2)}) %all-to-all-start.2) | async-done | bytes 24608 | tf_op jit(solution)/shard_map/all_to_all | solution.py:32
  196.9 4.7 %all-to-all-start.3 = ((bf16[16,704,128]{2,1,0:T(8,128)(2,1)}), bf16[16,704,128]{2,1,0:T(8,128)(2,1)}, u32[]{:S(2)}, u32[]{:S(2)}) async-start(bf16[16,704,128]{2,1,0:T(8,128)(2,1)} %stack.2), calls=%async_computation.3 | async-start | bytes 5767168 | tf_op jit(solution)/shard_map/all_to_all | solution.py:176
  201.6 18.6 %all-gather.6.cloned.1.call-done = bf16[768,2048]{0,1:T(8,128)(2,1)} async-done(((bf16[768,256]{0,1:T(8,128)(2,1)}), bf16[768,2048]{0,1:T(8,128)(2,1)}) %all-gather.6.cloned.1.call-update) | async-done | bytes 3145744 | tf_op jit(solution)/shard_map/all_gather | solution.py:168
  220.2 5.2 %fusion.18 = f32[768,704]{0,1:T(8,128)S(1)} fusion(bf16[768,2048]{0,1:T(8,128)(2,1)} %all-gather.6.cloned.1.call-done, bf16[2048,1408]{0,1:T(8,128)(2,1)} %all-gather.8.cloned.1.call-done), kind=kOutput, calls=%fused_computation.24 | convolution fusion | flops 2214592512 | bytes 8192000 | tf_op jit(solution)/shard_map/dot_general | solution.py:170
  225.4 18.9 %all-to-all-done.3 = bf16[16,704,128]{2,1,0:T(8,128)(2,1)} async-done(((bf16[16,704,128]{2,1,0:T(8,128)(2,1)}), bf16[16,704,128]{2,1,0:T(8,128)(2,1)}, u32[]{:S(2)}, u32[]{:S(2)}) %all-to-all-start.3) | async-done | bytes 2883616 | tf_op jit(solution)/shard_map/all_to_all | solution.py:176
  244.3 11.8 %convolution_convert_fusion = bf16[768,2048]{1,0:T(8,128)(2,1)} fusion(f32[768,704]{0,1:T(8,128)S(1)} %fusion.18, bf16[768,2048]{0,1:T(8,128)(2,1)} %all-gather.6.cloned.1.call-done, bf16[2048,1408]{0,1:T(8,128)(2,1)} %all-gather.8.cloned.1.call-done, bf16[16,704,128]{2,1,0:T(8,128)(2,1)} %all-to-all-done.3), kind=kOutput, calls=%fused_computation.18 | convolution fusion | flops 4434001920 | bytes 14221312 | tf_op jit(solution)/shard_map/dot_general | solution.py:173
  258.1 41.7 %all_to_all.37 = bf16[8,768,256]{2,1,0:T(8,128)(2,1)S(1)} all-to-all(bf16[8,768,256]{2,1,0:T(8,128)(2,1)S(1)} %bitcast.73), channel_id=1, replica_groups=mesh['sp'=16,'tp'=8] {'tp'}, dimensions={0} | all-to-all | bytes 6291456 | tf_op jit(solution)/shard_map/all_to_all | solution.py:52
  (92 shorter events, 27.2 us)
Async XLA Ops:
  6.5 2.4 copy-start
  6.5 71.7 %all-gather.4.cloned.1.call-start = ((), (), s32[]{:S(2)}) async-start(), calls=%async_computation.5 | async-start | bytes 6684672 | tf_op jit(solution)/shard_map/all_gather | solution.py:21
  10.5 3.1 %copy-start.3 = (bf16[128,2048]{1,0:T(8,128)(2,1)S(1)}, bf16[128,2048]{1,0:T(8,128)(2,1)}, u32[]{:S(2)}) copy-start(bf16[128,2048]{1,0:T(8,128)(2,1)} %param.19) | copy-start | bytes 1572868
  12.3 8.1 %copy-start.4 = (bf16[128,704]{0,1:T(8,128)(2,1)S(1)}, bf16[128,704]{0,1:T(8,128)(2,1)}, u32[]{:S(2)}) copy-start(bf16[128,704]{0,1:T(8,128)(2,1)} %param.22) | copy-start | bytes 540676
  12.3 8.1 %copy-start.5 = (bf16[128,704]{0,1:T(8,128)(2,1)S(1)}, bf16[128,704]{0,1:T(8,128)(2,1)}, u32[]{:S(2)}) copy-start(bf16[128,704]{0,1:T(8,128)(2,1)} %param.21) | copy-start | bytes 540676
  14.6 140.2 %all-to-all-start.1 = ((bf16[128,8,256]{0,2,1:T(8,128)(2,1)}), bf16[128,8,256]{0,2,1:T(8,128)(2,1)S(1)}, u32[]{:S(2)}, u32[]{:S(2)}) async-start(bf16[128,8,256]{0,2,1:T(8,128)(2,1)} %bitcast.9), calls=%async_computation.1 | async-start | bytes 1048576 | tf_op jit(solution)/shard_map/all_to_all | solution.py:100
  20.4 181.2 %all-gather.8.cloned.1.call-start = ((), (), s32[]{:S(2)}) async-start(), calls=%async_computation.7 | async-start | bytes 6127616 | tf_op jit(solution)/shard_map/all_gather | solution.py:21
  87.6 5.0 %copy-start.1 = (f32[2048,768]{1,0:T(8,128)S(1)}, f32[2048,768]{1,0:T(8,128)}, u32[]{:S(2)}) copy-start(f32[2048,768]{1,0:T(8,128)} %get-tuple-element.238) | copy-start | bytes 18874372 | tf_op jit(solution)/shard_map/while
  99.6 4.7 %copy-start.1 = (f32[2048,768]{1,0:T(8,128)S(1)}, f32[2048,768]{1,0:T(8,128)}, u32[]{:S(2)}) copy-start(f32[2048,768]{1,0:T(8,128)} %get-tuple-element.238) | copy-start | bytes 18874372 | tf_op jit(solution)/shard_map/while
  111.4 5.0 %copy-start.1 = (f32[2048,768]{1,0:T(8,128)S(1)}, f32[2048,768]{1,0:T(8,128)}, u32[]{:S(2)}) copy-start(f32[2048,768]{1,0:T(8,128)} %get-tuple-element.238) | copy-start | bytes 18874372 | tf_op jit(solution)/shard_map/while
  123.5 5.0 %copy-start.1 = (f32[2048,768]{1,0:T(8,128)S(1)}, f32[2048,768]{1,0:T(8,128)}, u32[]{:S(2)}) copy-start(f32[2048,768]{1,0:T(8,128)} %get-tuple-element.238) | copy-start | bytes 18874372 | tf_op jit(solution)/shard_map/while
  135.6 4.9 %copy-start.1 = (f32[2048,768]{1,0:T(8,128)S(1)}, f32[2048,768]{1,0:T(8,128)}, u32[]{:S(2)}) copy-start(f32[2048,768]{1,0:T(8,128)} %get-tuple-element.238) | copy-start | bytes 18874372 | tf_op jit(solution)/shard_map/while
  147.5 4.6 %copy-start.1 = (f32[2048,768]{1,0:T(8,128)S(1)}, f32[2048,768]{1,0:T(8,128)}, u32[]{:S(2)}) copy-start(f32[2048,768]{1,0:T(8,128)} %get-tuple-element.238) | copy-start | bytes 18874372 | tf_op jit(solution)/shard_map/while
  156.2 25.8 %all-to-all-start = ((bf16[8,768,128]{1,2,0:T(8,128)(2,1)}), bf16[8,768,128]{1,2,0:T(8,128)(2,1)S(1)}, u32[]{:S(2)}, u32[]{:S(2)}) async-start(bf16[8,768,128]{1,2,0:T(8,128)(2,1)} %broadcast_in_dim.17), calls=%async_computation | async-start | bytes 3145728 | tf_op jit(solution)/shard_map/all_to_all | solution.py:32
  183.0 1.0 copy-start.2
  183.5 11.2 %copy-start.6 = (bf16[704,128]{1,0:T(8,128)(2,1)S(1)}, bf16[704,128]{1,0:T(8,128)(2,1)}, u32[]{:S(2)}) copy-start(bf16[704,128]{1,0:T(8,128)(2,1)} %param.23) | copy-start | bytes 540676
  184.9 8.9 %all-to-all-start.2 = ((f32[8,1,768]{2,1,0:T(1,128)}), f32[8,1,768]{2,1,0:T(1,128)S(1)}, u32[]{:S(2)}, u32[]{:S(2)}) async-start(f32[8,1,768]{2,1,0:T(1,128)} %broadcast_in_dim.18), calls=%async_computation.2 | async-start | bytes 49152 | tf_op jit(solution)/shard_map/all_to_all | solution.py:32
  189.1 31.1 %all-gather.6.cloned.1.call-start = ((), (), s32[]{:S(2)}) async-start(), calls=%async_computation.6 | async-start | bytes 3538944 | tf_op jit(solution)/shard_map/all_gather | solution.py:168
  196.9 47.4 %all-to-all-start.3 = ((bf16[16,704,128]{2,1,0:T(8,128)(2,1)}), bf16[16,704,128]{2,1,0:T(8,128)(2,1)}, u32[]{:S(2)}, u32[]{:S(2)}) async-start(bf16[16,704,128]{2,1,0:T(8,128)(2,1)} %stack.2), calls=%async_computation.3 | async-start | bytes 5767168 | tf_op jit(solution)/shard_map/all_to_all | solution.py:176
Sparse Core Ops, SparseCore 0:
  13.7 64.4 all-gather.3
  80.3 62.8 all-gather.7
  194.9 25.3 all-gather.5
